TPU v7x, 512 devices: a whole 4x8x8 slice. The times are simulated.
512 devices in a mesh: ep: 32 (over z, x), tp: 16 (over y, core).
Axes of the slice: x: 4, y: 8, z: 8, core: 2. Of those that a mesh axis runs over, the one named last changes fastest.
Arguments:
- tokens: bfloat16 [256, 4096], P('ep', 'tp'), may hold values from -6 to 6
- norm_gain: float32 [4096], replicated, may hold values from 0.1 to 1.9
- route_experts: int32 [256, 2], P('ep'), may hold values from 0 to 63, all different within a row; in each aligned block of 8 rows (0 to 7, 8 to 15, ...) at most 2 rows name the same one
- route_logits: float32 [256, 2], P('ep'), may hold values from -4 to 4
- expert_gate: bfloat16 [64, 4096, 1024], P('ep', None, 'tp'), may hold values from -0.09375 to 0.09375
- expert_up: bfloat16 [64, 4096, 1024], P('ep', None, 'tp'), may hold values from -0.09375 to 0.09375
- expert_down: bfloat16 [64, 1024, 4096], P('ep', 'tp'), may hold values from -0.1875 to 0.1875
- dense_gate: bfloat16 [4096, 1024], P(None, 'tp'), may hold values from -0.09375 to 0.09375
- dense_up: bfloat16 [4096, 1024], P(None, 'tp'), may hold values from -0.09375 to 0.09375
- dense_down: bfloat16 [1024, 4096], P('tp'), may hold values from -0.1875 to 0.1875
- mix_weight: float32 [4096], replicated, may hold values from -0.09375 to 0.09375
- out_gain: float32 [4096], P('tp'), may hold values from 0.1 to 1.9
Outputs:
- result: bfloat16 [256, 4096], P('ep', 'tp')
Inputs may be any that keep to these rules, and one draw needn't show every extreme that they name: `route_experts`: each row names 2 different experts; the 8 rows of one index of ep (aligned blocks) name any one expert at most 2 times, and some block names some expert exactly 2 times; every expert is named somewhere.
All inputs are finite; a program needn't handle non-finite values.
Results may differ from a plain program's by a relative error of at most 0.0025.
Values may be sent and summed in bfloat16 or wider, within the bound.
A program may use at most 64 MiB of HBM per device.

v0:
```python
import jax
import jax.numpy as jnp
from jax import lax
from jax.sharding import Mesh
from jax.sharding import PartitionSpec as P

CAP = 2
TP = ("tp_0", "tp_1")


norm_eps = 1e-06


def summed_rows(x, axes, dim):
    if not axes:
        return x
    nearer = lax.psum_scatter(x, axes[0], scatter_dimension=dim, tiled=True)
    return summed_rows(nearer, axes[1:], dim)


def local(
    tokens,
    norm_gain,
    route_experts,
    route_logits,
    expert_gate,
    expert_up,
    expert_down,
    dense_gate,
    dense_up,
    dense_down,
    mix_weight,
    out_gain,
):
    tok_rows, width_part = tokens.shape
    groups = lax.axis_size(TP)
    width = width_part * groups
    whole_rows = lax.all_gather(tokens, TP, axis=1, tiled=True).astype(jnp.float32)
    normed = (
        whole_rows
        * lax.rsqrt(jnp.mean(whole_rows * whole_rows, axis=1, keepdims=True) + norm_eps)
        * norm_gain
    ).astype(jnp.bfloat16)
    weights = jax.nn.softmax(route_logits, axis=-1)
    top_count = route_experts.shape[1]
    local_experts = expert_gate.shape[0]
    peer_count = lax.axis_size("ep")
    experts = local_experts * peer_count
    dense_hidden = (
        jax.nn.silu(jnp.dot(normed, dense_gate, preferred_element_type=jnp.float32))
        * jnp.dot(normed, dense_up, preferred_element_type=jnp.float32)
    ).astype(jnp.bfloat16)
    dense_out = summed_rows(
        jnp.dot(dense_hidden, dense_down, preferred_element_type=jnp.float32), TP, 1
    )
    mix_gate = jax.nn.sigmoid(
        jnp.dot(normed.astype(jnp.float32), mix_weight, precision=lax.Precision.HIGHEST)
    )
    flat_routes = route_experts.reshape(-1)
    expert_ids = jnp.arange(experts, dtype=jnp.int32)
    capacity = CAP
    slot_count = experts * capacity
    route_hits = (flat_routes[:, None] == expert_ids[None, :]).astype(jnp.int32)
    before = jnp.cumsum(route_hits, axis=0) - route_hits
    slot_rank = jnp.sum(before * route_hits, axis=1)
    position = flat_routes * capacity + slot_rank
    onehot_place = (position[:, None] == jnp.arange(slot_count, dtype=jnp.int32)[None, :]).astype(
        jnp.float32
    )
    placing = jnp.sum(onehot_place.reshape(tok_rows, top_count, slot_count), axis=1).T.astype(
        jnp.bfloat16
    )
    outgoing = jnp.dot(placing, normed, preferred_element_type=jnp.float32).astype(jnp.bfloat16)
    received = lax.all_to_all(outgoing, "ep", split_axis=0, concat_axis=0, tiled=True)
    arranged = (
        received.reshape(peer_count, local_experts, capacity, width)
        .transpose(1, 0, 2, 3)
        .reshape(local_experts, peer_count * capacity, width)
    )
    gate_act = jnp.einsum("erd,edf->erf", arranged, expert_gate, preferred_element_type=jnp.float32)
    up_act = jnp.einsum("erd,edf->erf", arranged, expert_up, preferred_element_type=jnp.float32)
    hidden = (jax.nn.silu(gate_act) * up_act).astype(jnp.bfloat16)
    partial_value = jnp.einsum(
        "erf,efd->erd", hidden, expert_down, preferred_element_type=jnp.float32
    )
    summed = lax.psum_scatter(partial_value, TP, scatter_dimension=2, tiled=True)
    back_send = (
        summed.reshape(local_experts, peer_count, capacity, width_part)
        .transpose(1, 0, 2, 3)
        .reshape(slot_count, width_part)
    )
    returned = lax.all_to_all(back_send, "ep", split_axis=0, concat_axis=0, tiled=True)
    combine_map = jnp.sum(
        (onehot_place * weights.reshape(-1)[:, None]).reshape(tok_rows, top_count, slot_count),
        axis=1,
    )
    expert_mix = jnp.dot(combine_map, returned, precision=lax.Precision.HIGHEST)
    combined = expert_mix + mix_gate[:, None] * dense_out
    squares_out = lax.psum(jnp.sum(combined * combined, axis=1), TP)
    result = combined * lax.rsqrt(squares_out[:, None] / width + norm_eps) * out_gain
    return result.astype(jnp.bfloat16)


def solution(mesh):
    split = Mesh(mesh.devices.reshape(mesh.shape["ep"], 8, 2), ("ep", "tp_0", "tp_1"))
    in_specs = (
        P("ep", TP),
        P(),
        P("ep", None),
        P("ep", None),
        P("ep", None, TP),
        P("ep", None, TP),
        P("ep", TP, None),
        P(None, TP),
        P(None, TP),
        P(TP, None),
        P(),
        P(TP),
    )
    out_specs = P("ep", TP)
    return jax.shard_map(local, mesh=split, in_specs=in_specs, out_specs=out_specs, check_vma=False)
```

profile of v0, /device:TPU:1, one launch (start us, length us, event | category | flops | bytes accessed | tf_op | source)
XLA Modules:
  0.0 228.6 jit_solution(5264460515615627035)
XLA Ops:
  6.5 0.8 reduce_max.9
  7.3 0.7 fusion.26
  8.0 0.7 fusion.25
  8.7 0.8 copy.34
  10.0 21.2 %all_gather.3 = bf16[8,4096]{1,0:T(8,128)(2,1)S(1)} all-gather(bf16[8,256]{1,0:T(8,128)(2,1)} %param.12), channel_id=1, replica_groups=mesh['ep'=32,'tp_0'=8,'tp_1'=2] {'tp_0','tp_1'}, dimensions={1}, use_global_device_ids=true | all-gather | bytes 69632 | tf_op jit(solution)/shard_map/all_gather | solution.py:38
  31.4 1.2 convolution_convert_fusion
  32.7 0.4 all_to_all.14
  33.1 37.3 %all_to_all.21 = bf16[32,4,4096]{2,1,0:T(4,128)(2,1)S(1)} all-to-all(bf16[32,4,4096]{2,1,0:T(4,128)(2,1)S(1)} %all_to_all.14), channel_id=1, replica_groups=mesh['ep'=32,'tp_0'=8,'tp_1'=2] {'ep'}, dimensions={0} | all-to-all | bytes 2097152 | tf_op jit(solution)/shard_map/all_to_all | solution.py:74
  70.4 0.5 reshape.67
  70.9 2.0 copy.41
  73.0 1.6 reshape.68
  74.5 0.4 fusion.35
  75.0 3.4 %fusion.1 = f32[2,64,4096]{2,1,0:T(8,128)} fusion(bf16[2,64,4096]{2,1,0:T(8,128)(2,1)S(1)} %copy-done, bf16[2,64,4096]{2,1,0:T(8,128)(2,1)S(1)} %reshape.68, bf16[2,4096,64]{1,2,0:T(8,128)(2,1)} %param.17, f32[2,64,64]{2,1,0:T(8,128)S(1)} %fusion.35), kind=kOutput, calls=%fused_computation.3 | convolution fusion | flops 134266880 | bytes 5275648 | tf_op jit(solution)/shard_map/erf,efd->erd/dot_general | solution.py:83
  78.5 0.9 copy-done.2
  79.7 1.3 fusion.3
  81.0 55.0 %reduce-scatter.4.cloned.1.call-done = f32[2,64,256]{2,1,0:T(8,128)} async-done(((f32[2,64,4096]{2,1,0:T(8,128)}), f32[2,64,256]{2,1,0:T(8,128)}) %reduce-scatter.4.cloned.1.call-update) | async-done | bytes 131088 | tf_op jit(solution)/shard_map/reduce_scatter | solution.py:86
  136.0 1.0 reshape.69
  137.0 0.7 copy.39
  137.7 8.9 %all-to-all-start.1 = ((f32[32,4,256]{2,1,0:T(4,128)}), f32[32,4,256]{2,1,0:T(4,128)S(1)}, u32[]{:S(2)}, u32[]{:S(2)}) async-start(f32[32,4,256]{2,1,0:T(4,128)} %copy.39), calls=%async_computation.2 | async-start | bytes 262144 | tf_op jit(solution)/shard_map/all_to_all | solution.py:92
  146.7 26.9 %reduce-scatter.6.cloned.1.call-done = f32[8,512]{1,0:T(8,128)} async-done(((f32[8,4096]{1,0:T(8,128)}), f32[8,512]{1,0:T(8,128)}) %reduce-scatter.6.cloned.1.call-update) | async-done | bytes 16400 | tf_op jit(solution)/shard_map/reduce_scatter | solution.py:17
  174.0 23.7 %reduce-scatter.8.cloned.1.call-done = f32[8,256]{1,0:T(8,128)} async-done(((f32[8,512]{1,0:T(8,128)}), f32[8,256]{1,0:T(8,128)}) %reduce-scatter.8.cloned.1.call-update) | async-done | bytes 8208 | tf_op jit(solution)/shard_map/reduce_scatter | solution.py:17
  197.7 1.0 multiply_reduce_fusion
  198.7 22.7 %psum.7 = f32[8]{0:T(128)S(1)} all-reduce(f32[8]{0:T(128)S(1)} %get-tuple-element.7), channel_id=1, replica_groups=mesh['ep'=32,'tp_0'=8,'tp_1'=2] {'tp_0','tp_1'}, use_global_device_ids=true, to_apply=%region_11.12 | all-reduce | flops 8 | bytes 64 | tf_op jit(solution)/shard_map/psum | solution.py:99
  221.4 0.7 multiply_convert_fusion
  (37 shorter events, 1.7 us)
Async XLA Ops:
  6.5 68.4 %copy-start = (bf16[2,64,4096]{2,1,0:T(8,128)(2,1)S(1)}, bf16[2,64,4096]{2,1,0:T(8,128)(2,1)}, u32[]{:S(2)}) copy-start(bf16[2,64,4096]{2,1,0:T(8,128)(2,1)} %param.18) | copy-start | bytes 3145732
  6.5 129.4 %reduce-scatter.4.cloned.1.call-start = ((), (), s32[]{:S(2)}) async-start(), calls=%async_computation.5 | async-start | bytes 2228224 | tf_op jit(solution)/shard_map/reduce_scatter | solution.py:86
  73.0 1.6 copy-start.1
  78.4 1.0 copy-start.2
  78.4 1.0 copy-start.5
  78.4 1.3 copy-start.3
  78.4 1.4 copy-start.4
  78.4 95.3 %copy-start.7 = (f32[4096]{0:T(1024)S(1)}, f32[4096]{0:T(1024)}, u32[]{:S(2)}) copy-start(f32[4096]{0:T(1024)} %param.22) | copy-start | bytes 49156
  78.4 143.0 %copy-start.6 = (f32[256]{0:T(256)S(1)}, f32[256]{0:T(256)}, u32[]{:S(2)}) copy-start(f32[256]{0:T(256)} %param.23) | copy-start | bytes 3076
  78.4 95.2 %reduce-scatter.6.cloned.1.call-start = ((), (), s32[]{:S(2)}) async-start(), calls=%async_computation.6 | async-start | bytes 147456 | tf_op jit(solution)/shard_map/reduce_scatter | solution.py:17
  137.7 36.3 %all-to-all-start.1 = ((f32[32,4,256]{2,1,0:T(4,128)}), f32[32,4,256]{2,1,0:T(4,128)S(1)}, u32[]{:S(2)}, u32[]{:S(2)}) async-start(f32[32,4,256]{2,1,0:T(4,128)} %copy.39), calls=%async_computation.2 | async-start | bytes 262144 | tf_op jit(solution)/shard_map/all_to_all | solution.py:92
  146.6 51.1 %reduce-scatter.8.cloned.1.call-start = ((), (), s32[]{:S(2)}) async-start(), calls=%async_computation.7 | async-start | bytes 24576 | tf_op jit(solution)/shard_map/reduce_scatter | solution.py:17
Sparse Core Ops, SparseCore 0:
  78.5 57.4 reduce-scatter.3
  138.8 34.8 reduce-scatter.5
  176.3 21.3 reduce-scatter.7
where the time goes:
time: 230 us; the launch traced here: 229 us
  waiting for transfers between devices  106 us (46%)
  blocking collectives  81.2 us (35%)
  between operations  13.2 us (6%)
  starting transfers between devices  9 us (4%)
  local copies, waits for them, and re-layouts  8.3 us (4%)
  matrix products  7.81 us (3%)
  other arithmetic  3.38 us (1%)
    reduce_scatter x1, waiting for transfers between devices, local(): lax.psum_scatter(partial_value, TP, scatter_dimension=2, tiled=True)  55 us
    reduce_scatter x2, waiting for transfers between devices, summed_rows(): nearer = lax.psum_scatter(x, axes[0], scatter_dimension=dim, tiled=True)  50.6 us
    all_to_all x1, blocking collectives, local(): lax.all_to_all(outgoing, 'ep', split_axis=0, concat_axis=0, tiled=True)  37.3 us
    psum x1, blocking collectives, local(): squares_out = lax.psum(jnp.sum(combined * combined, axis=1), TP)  22.7 us
    all_gather x1, blocking collectives, local(): lax.all_gather(tokens, TP, axis=1, tiled=True).astype(jnp.float32)  21.2 us
    all_to_all x1, starting transfers between devices, local(): lax.all_to_all(back_send, 'ep', split_axis=0, concat_axis=0, tiled=True)  8.91 us
  transfers between devices with their start and end apart: 4, of which 3 were waited for; matrix products, arithmetic and copies ran while one was open for 2% of the time, Pallas kernels for 0%

commit v1 on v0

v1 whole, which is shorter than its diff:
```python
import functools

import jax
import jax.numpy as jnp
from jax import lax
from jax.experimental import pallas as pl
from jax.experimental.pallas import tpu as pltpu
from jax.sharding import PartitionSpec as P

MESH = pl.DeviceIdType.MESH
F32 = jnp.float32
BF16 = jnp.bfloat16
EPS = 1e-6
HIGHEST = lax.Precision.HIGHEST
NT = (((1,), (1,)), ((), ()))
NN = (((1,), (0,)), ((), ()))
RIGHT, LEFT = 0, 1


def step_kernel(
    n_ep,
    ny,
    tok_in, gain_in, routes_in, logits_in, eg_in, eu_in, ed_in, dg_in, du_in, dd_in, mixw_in, og_in,
    out_ref,
    tok, gain, routes, logits, wgu, wdown, dgu, ddown, mixw, og,
    send_a, land_a, xs, ym, yo, yp, ea, eb, send_f, land_f, sq_send, sq_land,
    in_sem, as_sem, ar_sem, bs_sem, br_sem, ds_sem, dr_sem, ps_sem, pr_sem, es_sem, er_sem,
    fs_sem, fr_sem, gs_sem, gr_sem,
):
    n_tp = 2 * ny
    half = n_ep // 2
    group = 4 * half
    ep = lax.axis_index("ep")
    tp = lax.axis_index("tp")
    y = tp // 2
    par = lax.rem(tp, 2)
    width = 256 * n_tp
    x_lo = group + 16
    y_lo = group + 8
    x_rows = (pl.ds(0, group + 16), pl.ds(x_lo, group))
    y_rows = (pl.ds(0, group + 8), pl.ds(y_lo, group))

    bar = pltpu.get_barrier_semaphore()

    def greet_ep(i, _):
        pl.semaphore_signal(bar, inc=1, device_id=(lax.rem(ep + i, n_ep), tp), device_id_type=MESH)
        return 0

    def greet_tp(i, _):
        pl.semaphore_signal(bar, inc=1, device_id=(ep, lax.rem(tp + i, n_tp)), device_id_type=MESH)
        return 0

    lax.fori_loop(1, n_ep, greet_ep, 0)
    lax.fori_loop(1, n_tp, greet_tp, 0)

    loads = [
        pltpu.make_async_copy(src, dst, in_sem.at[i])
        for i, (src, dst) in enumerate(
            [
                (tok_in, tok), (routes_in, routes), (logits_in, logits), (gain_in, gain), (mixw_in, mixw), (og_in, og),
                (eg_in, wgu.at[:, pl.ds(0, 64), :]), (eu_in, wgu.at[:, pl.ds(64, 64), :]),
                (dg_in, dgu.at[pl.ds(0, 64), :]), (du_in, dgu.at[pl.ds(64, 64), :]),
                (ed_in, wdown), (dd_in, ddown),
            ]
        )
    ]
    for load in loads:
        load.start()
    for load in loads[:3]:
        load.wait()

    lanes = 8 * n_ep
    eye = lax.broadcasted_iota(jnp.int32, (8, 8), 0) == lax.broadcasted_iota(jnp.int32, (8, 8), 1)

    def column(v):
        c = jnp.sum(jnp.where(eye, v, 0.0), axis=1, keepdims=True)
        return jnp.concatenate([c, c], axis=0)

    named = routes[...].astype(F32)
    first, second = column(named[0:1]), column(named[1:2])
    lg = logits[...]
    top = jnp.maximum(lg[0:1], lg[1:2])
    w0, w1 = jnp.exp(lg[0:1] - top), jnp.exp(lg[1:2] - top)
    whole = w0 + w1
    w0, w1 = column(w0 / whole), column(w1 / whole)
    lane = lax.broadcasted_iota(jnp.int32, (16, lanes), 1)
    row = lax.broadcasted_iota(jnp.int32, (16, lanes), 0)
    expert = (lane >> 2).astype(F32)
    hit0 = expert == first
    hit = jnp.where(hit0 | (expert == second), 1.0, 0.0)
    a = lax.broadcasted_iota(jnp.int32, (16, 16), 0)
    b = lax.broadcasted_iota(jnp.int32, (16, 16), 1)
    earlier = jnp.where(((a >> 3) == (b >> 3)) & ((b & 7) < (a & 7)), 1.0, 0.0)
    rank = lax.dot_general(earlier, hit, NN, preferred_element_type=F32)
    placed = (hit > 0.5) & (rank == ((lane >> 1) & 1).astype(F32)) & ((lane & 1) == (row >> 3))
    place = jnp.where(placed, 1.0, 0.0)
    weigh = jnp.where(placed, jnp.where(hit0, w0, w1), 0.0)
    mine = tok[...].astype(F32)
    halves = jnp.concatenate([mine[:, :128], mine[:, 128:]], axis=0)
    send_a[...] = lax.dot_general(
        jnp.transpose(place).astype(BF16), halves.astype(BF16), NN, preferred_element_type=F32
    )
    pl.semaphore_wait(bar, n_ep + n_tp - 2)

    block = pl.multiple_of(8 * ep, 8)

    def to_peer(src, dst, s_sem, r_sem, peer):
        return pltpu.make_async_remote_copy(
            src_ref=src.at[pl.ds(pl.multiple_of(8 * peer, 8), 8), :],
            dst_ref=dst.at[pl.ds(block, 8), :],
            send_sem=s_sem.at[peer],
            recv_sem=r_sem.at[ep],
            device_id=(peer, tp),
            device_id_type=MESH,
        )

    def from_peer(src, dst, s_sem, r_sem, peer):
        return pltpu.make_async_remote_copy(
            src_ref=src.at[pl.ds(block, 8), :],
            dst_ref=dst.at[pl.ds(pl.multiple_of(8 * peer, 8), 8), :],
            send_sem=s_sem.at[peer],
            recv_sem=r_sem.at[peer],
            device_id=(peer, tp),
            device_id_type=MESH,
        )

    def send_one(i, _):
        to_peer(send_a, land_a, as_sem, ar_sem, lax.rem(ep + i, n_ep)).start()
        return 0

    lax.fori_loop(1, n_ep, send_one, 0)
    land_a[pl.ds(block, 8), :] = send_a[pl.ds(block, 8), :]
    own16 = jnp.concatenate([mine, jnp.zeros_like(mine)], axis=0).astype(BF16)
    xs[tp, pl.ds(group, 16), :] = own16

    def wait_one(i, _):
        from_peer(send_a, land_a, as_sem, ar_sem, lax.rem(ep + i, n_ep)).wait_recv()
        return 0

    lax.fori_loop(1, n_ep, wait_one, 0)
    for part in range(2):
        for j in range(8):
            xs[tp, pl.ds((x_lo if part else 0) + (j // 2) * half, half), pl.ds((j % 2) * 128, 128)] = land_a[
                pl.ds(part * half * 8 + j, half, stride=8), :
            ].astype(BF16)

    right = (ep, lax.rem(y + 1, ny) * 2 + par)
    left = (ep, lax.rem(y + ny - 1, ny) * 2 + par)
    partner = (ep, y * 2 + (1 - par))
    far = ny // 2

    def slice_of(delta, parity):
        return lax.rem(y + delta, ny) * 2 + parity

    def ring_x(way, q, part, sending):
        age = q - 1 if sending else q
        delta = (ny - age) % ny if way == RIGHT else age % ny
        ref = xs.at[slice_of(delta, par), x_rows[part], :]
        return pltpu.make_async_remote_copy(
            src_ref=ref, dst_ref=ref, send_sem=bs_sem.at[way, q, part], recv_sem=br_sem.at[way, q, part],
            device_id=right if way == RIGHT else left, device_id_type=MESH,
        )

    def pair_x(delta, part, parity):
        ref = xs.at[slice_of(delta, parity), x_rows[part], :]
        return pltpu.make_async_remote_copy(
            src_ref=ref, dst_ref=ref, send_sem=ds_sem.at[delta, part], recv_sem=dr_sem.at[delta, part],
            device_id=partner, device_id_type=MESH,
        )

    sent = []

    def start(copy):
        copy.start()
        sent.append(copy)

    for part in (0, 1):
        start(ring_x(RIGHT, 1, part, True))
        start(ring_x(LEFT, 1, 1 - part, True))
    for part in (0, 1):
        start(pair_x(0, part, par))
    for q in range(1, far + 1):
        for turn in (0, 1):
            for way in (RIGHT, LEFT):
                part = turn if way == RIGHT else 1 - turn
                if q == far and turn:
                    continue
                ring_x(way, q, part, False).wait_recv()
                if q < far - 1 or (q == far - 1 and turn == 0):
                    start(ring_x(way, q + 1, part, True))
                start(pair_x((ny - q) % ny if way == RIGHT else q % ny, part, par))
    for load in loads[3:]:
        load.wait()
    for delta in range(ny):
        for part in (0, 1):
            pair_x(delta, part, 1 - par).wait_recv()

    n_rows = 2 * group + 16

    def squares(k, acc):
        v = xs[k].astype(F32)
        lo, hi = v[:, :128], v[:, 128:]
        return acc + (lo * lo + hi * hi)

    total = lax.fori_loop(0, n_tp, squares, jnp.zeros((n_rows, 128), F32))
    scale = lax.rsqrt(jnp.sum(total, axis=1, keepdims=True) / width + EPS)
    side = 2 * half

    def project(k, carry):
        e0, e1, dn, mg = carry
        v = xs[k].astype(F32) * scale
        lo = v[:, :128] * gain[pl.ds(2 * k, 1), :]
        hi = v[:, 128:] * gain[pl.ds(2 * k + 1, 1), :]
        nrm = jnp.concatenate([lo, hi], axis=1).astype(BF16)
        cols = pl.ds(pl.multiple_of(k * 256, 256), 256)
        r0 = jnp.concatenate([nrm[0:side], nrm[x_lo : x_lo + side]], axis=0)
        r1 = jnp.concatenate([nrm[side : 2 * side], nrm[x_lo + side : x_lo + 2 * side]], axis=0)
        rd = nrm[group : group + 16]
        e0 = e0 + lax.dot_general(r0, wgu[0, :, cols], NT, preferred_element_type=F32)
        e1 = e1 + lax.dot_general(r1, wgu[1, :, cols], NT, preferred_element_type=F32)
        dn = dn + lax.dot_general(rd, dgu[:, cols], NT, preferred_element_type=F32)
        d32 = rd.astype(F32)
        mg = mg + d32[0:8, :128] * mixw[pl.ds(2 * k, 1), :] + d32[0:8, 128:] * mixw[pl.ds(2 * k + 1, 1), :]
        return e0, e1, dn, mg

    e0, e1, dn, mg = lax.fori_loop(
        0, n_tp, project,
        (
            jnp.zeros((2 * side, 128), F32), jnp.zeros((2 * side, 128), F32), jnp.zeros((16, 128), F32),
            jnp.zeros((8, 128), F32),
        ),
    )

    def hidden(v):
        g = v[:, :64]
        return (g / (1.0 + jnp.exp(-g)) * v[:, 64:]).astype(BF16)

    h0, h1, hd = hidden(e0), hidden(e1), hidden(dn)
    mix_gate = 1.0 / (1.0 + jnp.exp(-jnp.sum(mg, axis=1, keepdims=True)))

    def down(i, parity):
        delta = lax.rem(far + i, ny)
        cols = pl.ds(pl.multiple_of(slice_of(delta, parity) * 256, 256), 256)
        o0 = lax.dot_general(h0, wdown[0, :, cols], NN, preferred_element_type=F32)
        o1 = lax.dot_general(h1, wdown[1, :, cols], NN, preferred_element_type=F32)
        od = lax.dot_general(hd, ddown[:, cols], NN, preferred_element_type=F32)
        return delta, o0, o1, od

    def fill(ref, delta, o0, o1, od):
        ref[delta, pl.ds(0, side), :] = o0[:side]
        ref[delta, pl.ds(side, side), :] = o1[:side]
        ref[delta, pl.ds(group, 8), :] = od[:8]
        ref[delta, pl.ds(y_lo, side), :] = o0[side:]
        ref[delta, pl.ds(y_lo + side, side), :] = o1[side:]

    def pair_y(delta):
        return pltpu.make_async_remote_copy(
            src_ref=yo.at[delta], dst_ref=yp.at[delta], send_sem=ps_sem.at[delta], recv_sem=pr_sem.at[delta],
            device_id=partner, device_id_type=MESH,
        )

    def produce(i, _):
        fill(yo, *down(i, 1 - par))
        pair_y(lax.rem(far + i, ny)).start()
        fill(ym, *down(i, par))
        return 0

    lax.fori_loop(0, ny, produce, 0)

    lands = (ea, eb)

    def ring_y(way, q, part):
        delta = q % ny if way == RIGHT else (ny - q) % ny
        return pltpu.make_async_remote_copy(
            src_ref=ym.at[delta, y_rows[part], :], dst_ref=lands[part].at[way, q],
            send_sem=es_sem.at[way, q, part], recv_sem=er_sem.at[way, q, part],
            device_id=right if way == RIGHT else left, device_id_type=MESH,
        )

    def gather(delta, part, came):
        v = ym[delta, y_rows[part], :] + yp[delta, y_rows[part], :]
        for way, q in came:
            ring_y(way, q, part).wait_recv()
            v = v + lands[part][way, q]
        ym[delta, y_rows[part], :] = v

    for q in range(far, 0, -1):
        for delta in sorted({q % ny, (ny - q) % ny}):
            pair_y(delta).wait_recv()
        for turn in (1, 0) if q < far else (0,):
            for way in (RIGHT, LEFT):
                part = turn if way == RIGHT else 1 - turn
                delta = q % ny if way == RIGHT else (ny - q) % ny
                have = q + 1 < far or (q + 1 == far and turn == 0)
                gather(delta, part, [(way, q + 1)] if have else [])
                start(ring_y(way, q, part))
    pair_y(0).wait_recv()

    for part in (1, 0):
        gather(0, part, [(RIGHT, 1), (LEFT, 1)])
        lo = y_lo if part else 0
        for j in range(8):
            send_f[pl.ds(part * half * 8 + j, half, stride=8), :] = ym[
                0, pl.ds(lo + (j // 2) * half, half), pl.ds((j % 2) * 128, 128)
            ]

        def send_back(i, _, part=part):
            peer = part * half + lax.rem(ep + i, half)

            @pl.when(peer != ep)
            def _():
                to_peer(send_f, land_f, fs_sem, fr_sem, peer).start()

            return 0

        lax.fori_loop(0, half, send_back, 0)
    land_f[pl.ds(block, 8), :] = send_f[pl.ds(block, 8), :]
    dense = ym[0, pl.ds(group, 8), :]
    dense16 = jnp.concatenate([dense[:, :128] * mix_gate, dense[:, 128:] * mix_gate], axis=0)

    def wait_back(i, _):
        from_peer(send_f, land_f, fs_sem, fr_sem, lax.rem(ep + i, n_ep)).wait_recv()
        return 0

    lax.fori_loop(1, n_ep, wait_back, 0)
    mixed = lax.dot_general(weigh, land_f[...], NN, precision=HIGHEST, preferred_element_type=F32) + dense16

    part_sq = jnp.sum(mixed[:8] * mixed[:8] + mixed[8:] * mixed[8:], axis=1, keepdims=True)
    diag = lax.broadcasted_iota(jnp.int32, (8, 128), 0) == lax.broadcasted_iota(jnp.int32, (8, 128), 1)
    sq_row = jnp.sum(jnp.where(diag, part_sq, 0.0), axis=0, keepdims=True)
    sq_send[...] = sq_row
    sq_land[tp] = sq_row

    def sq_copy(to, at):
        return pltpu.make_async_remote_copy(
            src_ref=sq_send, dst_ref=sq_land.at[at], send_sem=gs_sem.at[to], recv_sem=gr_sem.at[at],
            device_id=(ep, to), device_id_type=MESH,
        )

    def sq_start(i, _):
        sq_copy(lax.rem(tp + i, n_tp), tp).start()
        return 0

    def sq_wait(i, _):
        other = lax.rem(tp + i, n_tp)
        sq_copy(other, other).wait_recv()
        return 0

    lax.fori_loop(1, n_tp, sq_start, 0)
    lax.fori_loop(1, n_tp, sq_wait, 0)
    whole_sq = jnp.sum(jnp.sum(sq_land[...], axis=0), axis=0, keepdims=True)
    sq_col = jnp.sum(jnp.where(diag, whole_sq, 0.0), axis=1, keepdims=True)
    norm = lax.rsqrt(sq_col / width + EPS)
    out_ref[:, pl.ds(0, 128)] = (mixed[:8] * norm * og[0:1, :]).astype(BF16)
    out_ref[:, pl.ds(128, 128)] = (mixed[8:] * norm * og[1:2, :]).astype(BF16)

    for copy in sent:
        copy.wait_send()

    def drain_ep(i, _):
        peer = lax.rem(ep + i, n_ep)
        to_peer(send_a, land_a, as_sem, ar_sem, peer).wait_send()
        to_peer(send_f, land_f, fs_sem, fr_sem, peer).wait_send()
        return 0

    def drain_tp(i, _):
        sq_copy(lax.rem(tp + i, n_tp), tp).wait_send()
        return 0

    def drain_pair(i, _):
        pair_y(i).wait_send()
        return 0

    lax.fori_loop(1, n_ep, drain_ep, 0)
    lax.fori_loop(1, n_tp, drain_tp, 0)
    lax.fori_loop(0, ny, drain_pair, 0)


def local(
    n_ep, n_tp,
    tokens, norm_gain, route_experts, route_logits, expert_gate, expert_up, expert_down,
    dense_gate, dense_up, dense_down, mix_weight, out_gain,
):
    ny = n_tp // 2
    half = n_ep // 2
    group = 4 * half
    width = n_tp * 256
    far = ny // 2
    vmem, dma = pltpu.VMEM, pltpu.SemaphoreType.DMA
    args = (
        tokens,
        norm_gain.reshape(width // 128, 128),
        route_experts.T,
        route_logits.T,
        jnp.swapaxes(expert_gate, 1, 2),
        jnp.swapaxes(expert_up, 1, 2),
        expert_down,
        dense_gate.T,
        dense_up.T,
        dense_down,
        mix_weight.reshape(width // 128, 128),
        out_gain.reshape(2, 128),
    )
    return pl.pallas_call(
        functools.partial(step_kernel, n_ep, ny),
        out_shape=jax.ShapeDtypeStruct((8, 256), BF16),
        in_specs=[pl.BlockSpec(memory_space=pl.ANY)] * len(args),
        out_specs=pl.BlockSpec(memory_space=pltpu.VMEM),
        scratch_shapes=[
            vmem((8, 256), BF16), vmem((width // 128, 128), F32), vmem((2, 8), jnp.int32), vmem((2, 8), F32),
            vmem((2, 128, width), BF16), vmem((2, 64, width), BF16), vmem((128, width), BF16), vmem((64, width), BF16),
            vmem((width // 128, 128), F32), vmem((2, 128), F32),
            vmem((8 * n_ep, 128), F32), vmem((8 * n_ep, 128), F32),
            vmem((n_tp, 2 * group + 16, 256), BF16),
            vmem((ny, 2 * group + 8, 256), F32), vmem((ny, 2 * group + 8, 256), F32), vmem((ny, 2 * group + 8, 256), F32),
            vmem((2, far + 1, group + 8, 256), F32), vmem((2, far + 1, group, 256), F32),
            vmem((8 * n_ep, 128), F32), vmem((8 * n_ep, 128), F32),
            vmem((1, 128), F32), vmem((n_tp, 1, 128), F32),
            dma((12,)), dma((n_ep,)), dma((n_ep,)),
            dma((2, far + 1, 2)), dma((2, far + 1, 2)), dma((ny, 2)), dma((ny, 2)), dma((ny,)), dma((ny,)),
            dma((2, far + 1, 2)), dma((2, far + 1, 2)),
            dma((n_ep,)), dma((n_ep,)), dma((n_tp,)), dma((n_tp,)),
        ],
        compiler_params=pltpu.CompilerParams(collective_id=0, has_side_effects=True),
        name="step",
    )(*args)


def solution(mesh):
    tp = "tp"
    in_specs = (
        P("ep", tp), P(), P("ep", None), P("ep", None),
        P("ep", None, tp), P("ep", None, tp), P("ep", tp, None),
        P(None, tp), P(None, tp), P(tp, None), P(), P(tp),
    )
    return jax.shard_map(
        functools.partial(local, mesh.shape["ep"], mesh.shape["tp"]),
        mesh=mesh, in_specs=in_specs, out_specs=P("ep", tp), check_vma=False,
    )
```

time: 230 us -> 75.2 us (0.33)
  waiting for transfers between devices: 106 us -> 0 us
  blocking collectives: 81.2 us -> 0 us
  Pallas kernels: 0 us -> 73.7 us
  between operations: 13.2 us -> 0.01 us
  starting transfers between devices: 9 us -> 0 us
  matrix products: 7.81 us -> 0 us
  local copies, waits for them, and re-layouts: 8.3 us -> 1.28 us
  other arithmetic: 3.38 us -> 0 us
    reduce_scatter x3 -> x0, waiting for transfers between devices: 106 us -> none  [the longest x1 55 us: local(): lax.psum_scatter(partial_value, TP, scatter_dimension=2, tiled=True)]
    pallas_call x0 -> x1, Pallas kernels: none -> 73.7 us  [local(): pl.pallas_call(functools.partial(step_kernel, n_ep, ny), out_shape=jax.Sh...]
    all_to_all x1 -> x0, blocking collectives: 37.3 us -> none  [local(): lax.all_to_all(outgoing, 'ep', split_axis=0, concat_axis=0, tiled=True)]
    psum x1 -> x0, blocking collectives: 22.7 us -> none  [local(): squares_out = lax.psum(jnp.sum(combined * combined, axis=1), TP)]
    all_gather x1 -> x0, blocking collectives: 21.2 us -> none  [local(): lax.all_gather(tokens, TP, axis=1, tiled=True).astype(jnp.float32)]
    all_to_all x1 -> x0, starting transfers between devices: 8.91 us -> none  [local(): lax.all_to_all(back_send, 'ep', split_axis=0, concat_axis=0, tiled=True)]
    dot_general x7 -> x0, matrix products: 7.81 us -> none  [the longest x1 3.39 us: local(): jnp.einsum('erf,efd->erd', hidden, expert_down, preferred_element_type=jn...]
    reshape x5 -> x0, local copies, waits for them, and re-layouts: 5.09 us -> none  [the longest x2 2.55 us: local(): received.reshape(peer_count, local_experts, capacity, width)]
  transfers between devices with their start and end apart: 4 -> 0, of which waited for: 3 -> 0; matrix products, arithmetic and copies ran while one was open for 2% -> 0% of each run, Pallas kernels for 0% -> 0%
where the time goes in v1:
time: 75.2 us; the launch traced here: 75 us
  Pallas kernels  73.7 us (98%)
  local copies, waits for them, and re-layouts  1.28 us (2%)
    pallas_call x1, Pallas kernels, local(): pl.pallas_call(functools.partial(step_kernel, n_ep, ny), out_shape=jax.Sh...  73.7 us

profile of v1, /device:TPU:1, one launch (start us, length us, event | category | flops | bytes accessed | tf_op | source)
XLA Modules:
  0.0 75.0 jit_solution(5739870935356698037)
XLA Ops:
  0.0 73.7 %step.1 = bf16[8,256]{1,0:T(8,128)(2,1)} custom-call(bf16[8,256]{1,0:T(8,128)(2,1)} %tok_in.1, f32[32,128]{1,0:T(8,128)} %bitcast.13, s32[2,8]{1,0:T(2,128)} %bitcast.15, f32[2,8]{1,0:T(2,128)} %bitcast.16, bf16[2,64,4096]{2,1,0:T(8,128)(2,1)} %bitcast.9, bf16[2,64,4096]{2,1,0:T(8,128)(2,1)} %bitcast.10, bf16[2,64,4096]{2,1,0:T(8,128)(2,1)} %ed_in.1, ...), custom_call_target="tpu_custom_call" | custom-call | tf_op jit(solution)/shard_map/step/pallas_call | solution.py:404
  73.7 1.3 %copy.14 = bf16[8,256]{1,0:T(8,128)(2,1)} copy(bf16[8,256]{1,0:T(8,128)(2,1)} %step.1) | data formatting | bytes 8192
